TPU v7x, 32 devices: a whole 2x2x4 slice. The times are simulated.
32 devices in a mesh: sp: 8 (over z, y), tp: 4 (over x, core).
Axes of the slice: x: 2, y: 2, z: 4, core: 2. Of those that a mesh axis runs over, the one named last changes fastest.
Arguments:
- queries: bfloat16 [1536, 2048], P('sp', 'tp'), may hold values from -100 to 100
- keys: bfloat16 [1536, 512], P('sp'), may hold values from -8 to 8
- values: bfloat16 [1536, 512], P('sp'), may hold values from -6 to 6
- diff_scale: float32 [8], P('tp'), may hold values from 0.3 to 0.8
- head_gain: float32 [256], replicated, may hold values from 0.1 to 1.9
- w_out: bfloat16 [2048, 2048], P('tp'), may hold values from -0.125 to 0.125
- residual: bfloat16 [1536, 2048], P(('sp', 'tp')), may hold values from -6 to 6
- norm_gain: float32 [2048], replicated, may hold values from 0.1 to 1.9
- route_ids: int32 [1536, 2], P(('sp', 'tp')), may hold values from 0 to 7, all different within a row; in each aligned block of 48 rows (0 to 47, 48 to 95, ...) at most 18 rows name the same one
- route_weights: float32 [1536, 2], P(('sp', 'tp')), may hold values from 0.2 to 1
- w_gate: bfloat16 [8, 2048, 3072], P('sp', None, 'tp'), may hold values from -0.125 to 0.125
- w_up: bfloat16 [8, 2048, 3072], P('sp', None, 'tp'), may hold values from -0.125 to 0.125
- w_down: bfloat16 [8, 3072, 2048], P('sp', 'tp'), may hold values from -0.109375 to 0.109375
Outputs:
- layer_out: bfloat16 [1536, 2048], P(('sp', 'tp'))
Inputs may be any that keep to these rules, and one draw needn't show every extreme that they name: `route_ids`: in each aligned block of 48 rows (the rows of one device), no expert is named more than 18 times, a bound that some block reaches; a row names 2 different experts.
All inputs are finite; a program needn't handle non-finite values.
Results may differ from a plain program's by a relative error of at most 0.014.
Values may be sent and summed in bfloat16 or wider, within the bound.
A program may use at most 128 MiB of HBM per device.

v0:
```python
import math
import jax
import jax.numpy as jnp
from jax import lax
from jax.sharding import PartitionSpec as P

KV_HEADS = 2
EPS = 1e-06
LOWEST = -1e30


def swapped(value, axis, apart):
    mask = 2**apart
    pairs = [(source, source ^ mask) for source in range(lax.axis_size(axis))]
    return lax.ppermute(value, axis, pairs)


def attend(carry, piece, q_heads):
    half = q_heads.shape[-1]
    scale = 1.0 / math.sqrt(half)
    high, total, acc = carry
    rows = piece.shape[0]
    for first in range(0, rows, 2048):
        count = min(2048, rows - first)
        k_block = piece[first : first + count, : 2 * half].reshape(count, 2, half)
        v_block = piece[first : first + count, 2 * half :]
        scores = (
            jnp.einsum("qhmd,kmd->qhmk", q_heads, k_block, preferred_element_type=jnp.float32)
            * scale
        )
        peak = jnp.maximum(high, jnp.max(scores, axis=-1))
        fade = jnp.exp(high - peak)
        weights = jnp.exp(scores - peak[..., None]).astype(jnp.bfloat16)
        total = total * fade + jnp.sum(weights, axis=-1, dtype=jnp.float32)
        acc = acc * fade[..., None] + jnp.einsum(
            "qhmk,kd->qhmd", weights, v_block, preferred_element_type=jnp.float32
        )
        high = peak
    return (high, total, acc)


def local(
    queries,
    keys,
    values,
    diff_scale,
    head_gain,
    w_out,
    residual,
    norm_gain,
    route_ids,
    route_weights,
    w_gate,
    w_up,
    w_down,
):
    q_rows = queries.shape[0]
    heads_dev = diff_scale.shape[0]
    half_dim = queries.shape[1] // (2 * heads_dev)
    q_heads = queries.reshape(q_rows, heads_dev, 2, half_dim)
    group_cols = keys.shape[1] // KV_HEADS
    value_cols = values.shape[1] // KV_HEADS
    group = lax.axis_index("tp") // (lax.axis_size("tp") // KV_HEADS)
    k_group = lax.dynamic_slice_in_dim(keys, group * group_cols, group_cols, 1)
    v_group = lax.dynamic_slice_in_dim(values, group * value_cols, value_cols, 1)
    joined = jnp.concatenate([k_group, v_group], axis=1)
    start_state = (
        jnp.full((q_rows, heads_dev, 2), LOWEST, jnp.float32),
        jnp.zeros((q_rows, heads_dev, 2), jnp.float32),
        jnp.zeros((q_rows, heads_dev, 2, value_cols), jnp.float32),
    )
    part_rows = joined.shape[0] // 2
    side = lax.axis_index("tp") % 2
    own_half = lax.dynamic_slice_in_dim(joined, side * part_rows, part_rows, 0)
    near = lax.all_gather(own_half, "sp", axis=0, tiled=True)
    far = swapped(near, "tp", 0)
    high, total, acc = attend(attend(start_state, near, q_heads), far, q_heads)
    mixed = (
        acc[:, :, 0] / total[:, :, 0:1]
        - diff_scale[None, :, None] * acc[:, :, 1] / total[:, :, 1:2]
    )
    mixed = mixed * lax.rsqrt(jnp.mean(mixed * mixed, axis=-1, keepdims=True) + EPS) * head_gain
    head_out = mixed.astype(jnp.bfloat16).reshape(q_rows, heads_dev * value_cols)
    rows_out = residual.shape[0]
    attended = lax.psum_scatter(
        jnp.dot(head_out, w_out, preferred_element_type=jnp.float32).astype(jnp.bfloat16),
        "tp",
        scatter_dimension=0,
        tiled=True,
    ).astype(jnp.float32)
    state = residual.astype(jnp.float32) + attended
    normed = (
        state * lax.rsqrt(jnp.mean(state * state, axis=-1, keepdims=True) + EPS) * norm_gain
    ).astype(jnp.bfloat16)
    experts = lax.axis_size("sp")
    top = route_ids.shape[1]
    width = normed.shape[1]
    capacity = max(2, 3 * rows_out * top // (2 * experts))
    flat_ids = route_ids.reshape(-1)
    onehot = (flat_ids[:, None] == jnp.arange(experts, dtype=jnp.int32)[None, :]).astype(jnp.int32)
    slot = jnp.sum((jnp.cumsum(onehot, axis=0) - onehot) * onehot, axis=1)
    dest = flat_ids * capacity + slot
    copies = jnp.repeat(normed, top, axis=0)
    outgoing = (
        jnp.zeros((experts * capacity, width), jnp.bfloat16)
        .at[dest]
        .set(copies)
        .reshape(experts, capacity, width)
    )
    gathered = lax.all_gather(
        lax.all_to_all(outgoing, "sp", split_axis=0, concat_axis=0, tiled=True),
        "tp",
        axis=0,
        tiled=True,
    )
    flat = gathered.reshape(-1, width)
    gate = jnp.dot(flat, w_gate[0], preferred_element_type=jnp.float32)
    up = jnp.dot(flat, w_up[0], preferred_element_type=jnp.float32)
    hidden = (jax.nn.silu(gate) * up).astype(jnp.bfloat16)
    partial_value = jnp.dot(hidden, w_down[0], preferred_element_type=jnp.float32).reshape(
        gathered.shape[0], gathered.shape[1], width
    )
    served = lax.psum_scatter(
        partial_value.astype(jnp.bfloat16), "tp", scatter_dimension=0, tiled=True
    )
    returned = lax.all_to_all(served, "sp", split_axis=0, concat_axis=0, tiled=True).reshape(
        experts * capacity, width
    )
    picked = returned[dest].reshape(rows_out, top, width)
    expert_sum = jnp.einsum("rt,rtd->rd", route_weights, picked.astype(jnp.float32))
    return (state + expert_sum).astype(jnp.bfloat16)


def solution(mesh):
    in_specs = (
        P("sp", "tp"),
        P("sp", None),
        P("sp", None),
        P("tp"),
        P(),
        P("tp", None),
        P(("sp", "tp"), None),
        P(),
        P(("sp", "tp"), None),
        P(("sp", "tp"), None),
        P("sp", None, "tp"),
        P("sp", None, "tp"),
        P("sp", "tp", None),
    )
    out_specs = P(("sp", "tp"), None)
    return jax.shard_map(local, mesh=mesh, in_specs=in_specs, out_specs=out_specs, check_vma=False)
```

profile of v0, /device:TPU:0, one launch (start us, length us, event | category | flops | bytes accessed | tf_op | source)
XLA Modules:
  0.0 259.2 jit_solution(16398461399570761725)
XLA Ops:
  6.6 1.1 constant_dynamic-slice_fusion
  7.8 36.0 %all_gather.6 = bf16[768,512]{1,0:T(8,128)(2,1)} all-gather(bf16[96,512]{1,0:T(8,128)(2,1)S(1)} %fusion.36), channel_id=1, replica_groups=mesh['sp'=8,'tp'=4] {'sp'}, dimensions={0}, use_global_device_ids=true | all-gather | bytes 884736 | tf_op jit(solution)/shard_map/all_gather | solution.py:75
  43.8 1.8 slice.34
  45.6 1.9 copy.43
  47.5 0.1 broadcast_bitcast_fusion.1
  47.6 0.6 copy.86
  48.2 2.9 %bitcast_reduce_fusion.1 = (f32[192,2,2]{0,1,2:T(2,128)S(1)}, f32[2,768,192,2]{1,2,3,0:T(8,128)}) fusion(bf16[768,2,128,1]{0,2,3,1:T(8,128)(2,1)} %bitcast.119, bf16[192,2,2,128]{3,2,1,0:T(2,128)(2,1)S(1)} %reshape.102), kind=kOutput, calls=%fused_computation.16 | convolution fusion | flops 152173824 | bytes 2952192 | tf_op jit(solution)/shard_map/qhmd,kmd->qhmk/dot_general | solution.py:28
  51.0 1.8 slice.36
  52.8 1.9 reshape.103
  54.6 1.6 bitcast_reduce_fusion
  56.2 0.6 convert_reduce_fusion
  56.9 1.0 copy-done.1
  57.9 0.6 convert_reduce_fusion.1
  58.6 1.5 fusion.18
  60.1 1.5 convolution_add_fusion
  61.6 0.9 copy-done.2
  62.4 0.8 slice_bitcast_fusion.4
  63.3 0.8 copy.77
  64.0 1.4 fusion.28
  65.5 0.8 copy.78
  66.2 1.3 copy.53
  67.5 0.8 copy.80
  68.3 0.3 copy.55
  68.6 0.8 copy.83
  69.4 0.1 copy.57
  69.6 0.3 mul.141
  69.9 1.3 div.58.clone
  71.2 1.2 div.62.clone
  72.5 2.6 %convolution_convert_fusion = bf16[192,2048]{1,0:T(8,128)(2,1)} fusion(bf16[512,2048]{1,0:T(8,128)(2,1)S(1)} %copy-done.15, f32[192,512]{1,0:T(8,128)S(1)} %bitcast.124, f32[192,512]{1,0:T(8,128)S(1)} %bitcast.126, f32[192,512]{1,0:T(8,128)S(1)} %bitcast.123, f32[192,512]{1,0:T(8,128)} %bitcast.122, f32[192,512]{1,0:T(8,128)S(1)} %bitcast.125, ...), kind=kOutput, calls=%fused_computation.10 | convolution fusion | flops 403734528 | bytes 4853760 | tf_op jit(solution)/shard_map/dot_general | solution.py:86
  75.2 0.1 copy.59
  75.3 0.1 eq.17
  75.4 0.1 fusion.37
  75.5 0.1 reduce_window_sum.11
  75.6 0.1 copy.58
  75.7 0.1 mul.150
  75.8 0.2 select_reduce_fusion
  76.0 23.4 %reduce-scatter.5.cloned.1.call-done = bf16[48,2048]{1,0:T(8,128)(2,1)} async-done(((bf16[192,2048]{1,0:T(8,128)(2,1)}), bf16[48,2048]{1,0:T(8,128)(2,1)}) %reduce-scatter.5.cloned.1.call-update) | async-done | bytes 196624 | tf_op jit(solution)/shard_map/reduce_scatter | solution.py:85
  99.4 1.1 multiply_reduce_fusion
  100.6 1.0 multiply_convert_fusion.1
  101.6 1.0 broadcast_in_dim.11
  102.6 1.9 reshape.121
  104.5 2.5 scatter_custom_fusion
  107.0 2.1 reshape.105
  109.1 25.5 %all_to_all.10 = bf16[8,18,2048]{2,1,0:T(8,128)(2,1)S(1)} all-to-all(bf16[8,18,2048]{2,1,0:T(8,128)(2,1)} %reshape.105), channel_id=1, replica_groups=mesh['sp'=8,'tp'=4] {'sp'}, dimensions={0} | all-to-all | bytes 1179648 | tf_op jit(solution)/shard_map/all_to_all | solution.py:111
  134.6 1.2 copy.60
  135.8 0.2 reduce-scatter.7.cloned.1.call-start
  136.0 22.0 %all-gather.2.cloned.1.call-done = bf16[32,18,2048]{2,0,1:T(8,128)(2,1)} async-done(((bf16[8,18,2048]{2,0,1:T(8,128)(2,1)}), bf16[32,18,2048]{2,0,1:T(8,128)(2,1)}) %all-gather.2.cloned.1.call-update) | async-done | bytes 2359312 | tf_op jit(solution)/shard_map/all_gather | solution.py:110
  158.1 4.7 %copy.61 = bf16[32,18,2048]{2,1,0:T(8,128)(2,1)} copy(bf16[32,18,2048]{2,0,1:T(8,128)(2,1)} %all-gather.2.cloned.1.call-done) | data formatting | bytes 4718592 | tf_op jit(solution)/shard_map/all_gather | solution.py:110
  162.7 4.3 %reshape.106 = bf16[576,2048]{1,0:T(8,128)(2,1)} reshape(bf16[32,18,2048]{2,1,0:T(8,128)(2,1)} %copy.61) | data formatting | bytes 4718592 | tf_op jit(solution)/shard_map/reshape | solution.py:116
  167.1 4.7 %fusion.4 = f32[576,768]{1,0:T(8,128)S(1)} fusion(bf16[576,2048]{1,0:T(8,128)(2,1)} %reshape.106, bf16[1,2048,768]{2,1,0:T(8,128)(2,1)} %param.23), kind=kOutput, calls=%fused_computation.6 | convolution fusion | flops 1811939328 | bytes 7274496 | tf_op jit(solution)/shard_map/dot_general | solution.py:117
  171.8 3.1 %multiply_convert_fusion = bf16[576,768]{1,0:T(8,128)(2,1)} fusion(f32[576,768]{1,0:T(8,128)S(1)} %fusion.4, bf16[576,2048]{1,0:T(8,128)(2,1)S(1)} %copy-done.3, bf16[1,2048,768]{2,1,0:T(8,128)(2,1)S(1)} %copy-done.14), kind=kOutput, calls=%fused_computation.21 | convolution fusion | flops 1814593536 | bytes 8159232 | tf_op jit(solution)/shard_map/dot_general | solution.py:118
  174.9 2.2 dot_general.36
  177.1 3.3 %fusion.9 = bf16[18,4,8,2048]{3,2,1,0:T(8,128)(2,1)S(1)} fusion(bf16[1,768,2048]{2,1,0:T(8,128)(2,1)S(1)} %copy-done, bf16[32,18,768]{2,1,0:T(8,128)(2,1)} %dot_general.36), kind=kOutput, calls=%fused_computation.9 | convolution fusion | flops 1813118976 | bytes 6389760 | tf_op jit(solution)/shard_map/dot_general | solution.py:120
  180.4 1.6 copy.79
  182.0 33.0 %reduce-scatter.7.cloned.1.call-done = bf16[8,36864]{1,0:T(8,128)(2,1)} async-done(((bf16[32,36864]{1,0:T(8,128)(2,1)}), bf16[8,36864]{1,0:T(8,128)(2,1)}) %reduce-scatter.7.cloned.1.call-update) | async-done | bytes 589840
  215.0 2.3 copy.63
  217.3 5.5 %all-to-all-start.1 = ((bf16[8,18,2048]{2,1,0:T(8,128)(2,1)}), bf16[8,18,2048]{2,1,0:T(8,128)(2,1)}, u32[]{:S(2)}, u32[]{:S(2)}) async-start(bf16[8,18,2048]{2,1,0:T(8,128)(2,1)} %copy.63), calls=%async_computation.2 | async-start | bytes 1572864 | tf_op jit(solution)/shard_map/all_to_all | solution.py:126
  222.8 0.7 copy.68
  223.5 19.4 %all-to-all-done.1 = bf16[8,18,2048]{2,1,0:T(8,128)(2,1)} async-done(((bf16[8,18,2048]{2,1,0:T(8,128)(2,1)}), bf16[8,18,2048]{2,1,0:T(8,128)(2,1)}, u32[]{:S(2)}, u32[]{:S(2)}) %all-to-all-start.1) | async-done | bytes 589856 | tf_op jit(solution)/shard_map/all_to_all | solution.py:126
  243.0 2.1 reshape.107
  245.1 3.1 %gather_fusion = bf16[96,2048]{1,0:T(8,128)(2,1)} fusion(bf16[144,2048]{1,0:T(8,128)(2,1)} %reshape.107, s32[1024]{0:T(1024)S(1)} %pad_clamp_fusion), kind=kCustom, calls=%fused_computation | custom fusion | bytes 786816 | tf_op jit(solution)/shard_map/gather | solution.py:129
  248.2 2.0 reshape.108
  250.3 1.5 fusion.42
  251.8 0.8 fusion.24
  (54 shorter events, 0.4 us)
Async XLA Ops:
  6.5 170.6 %copy-start = (bf16[1,768,2048]{2,1,0:T(8,128)(2,1)S(1)}, bf16[1,768,2048]{2,1,0:T(8,128)(2,1)}, u32[]{:S(2)}) copy-start(bf16[1,768,2048]{2,1,0:T(8,128)(2,1)} %param.25) | copy-start | bytes 9437188
  6.5 39.0 %copy-start.7 = (bf16[192,512]{1,0:T(8,128)(2,1)S(1)}, bf16[192,512]{1,0:T(8,128)(2,1)}, u32[]{:S(2)}) copy-start(bf16[192,512]{1,0:T(8,128)(2,1)} %param.13) | copy-start | bytes 589828
  6.5 41.0 %copy-start.11 = (f32[2]{0:T(128)S(1)}, f32[2]{0:T(128)}, u32[]{:S(2)}) copy-start(f32[2]{0:T(128)} %param.16) | copy-start | bytes 28
  6.5 41.0 %copy-start.12 = (f32[256]{0:T(256)S(1)}, f32[256]{0:T(256)}, u32[]{:S(2)}) copy-start(f32[256]{0:T(256)} %param.17) | copy-start | bytes 3076
  6.5 92.9 %reduce-scatter.5.cloned.1.call-start = ((), (), s32[]{:S(2)}) async-start(), calls=%async_computation.4 | async-start | bytes 983040 | tf_op jit(solution)/shard_map/reduce_scatter | solution.py:85
  43.8 7.3 %collective-permute-start = (bf16[768,512]{1,0:T(8,128)(2,1)}, bf16[768,512]{1,0:T(8,128)(2,1)}, u32[]{:S(2)}, u32[]{:S(2)}) collective-permute-start(bf16[768,512]{1,0:T(8,128)(2,1)} %all_gather.6), channel_id=1, source_target_pairs={{0,1},{1,0},{2,3},{3,2},{4,5},{5,4},{6,7},{7,6},{8,9},{9,8},{10,11... | collective-permute-start | bytes 2359304 | tf_op jit(solution)/shard_map/ppermute | solution.py:15
  56.2 1.7 copy-start.1
  61.6 0.9 copy-start.2
  68.6 3.8 %copy-start.10 = (f32[1,2,2,128]{3,1,2,0:T(2,128)S(1)}, f32[1,2,2,128]{3,1,2,0:T(2,128)}, u32[]{:S(2)}) copy-start(f32[1,2,2,128]{3,1,2,0:T(2,128)} %copy.86) | copy-start | bytes 6148
  69.5 2.9 %copy-start.6 = (f32[24,8,2,256]{3,1,2,0:T(8,128)S(1)}, f32[24,8,2,256]{3,1,2,0:T(8,128)}, u32[]{:S(2)}) copy-start(f32[24,8,2,256]{3,1,2,0:T(8,128)} %copy.83) | copy-start | bytes 1179652
  69.5 2.9 %copy-start.15 = (bf16[512,2048]{1,0:T(8,128)(2,1)S(1)}, bf16[512,2048]{1,0:T(8,128)(2,1)}, u32[]{:S(2)}) copy-start(bf16[512,2048]{1,0:T(8,128)(2,1)} %param.18) | copy-start | bytes 6291460
  72.4 2.7 %copy-start.9 = (s32[48,2]{0,1:T(2,128)S(1)}, s32[48,2]{0,1:T(2,128)}, u32[]{:S(2)}) copy-start(s32[48,2]{0,1:T(2,128)} %param.21) | copy-start | bytes 1156
  72.5 27.0 %copy-start.4 = (bf16[48,2048]{1,0:T(8,128)(2,1)S(1)}, bf16[48,2048]{1,0:T(8,128)(2,1)}, u32[]{:S(2)}) copy-start(bf16[48,2048]{1,0:T(8,128)(2,1)} %param.19) | copy-start | bytes 589828
  72.5 28.1 %copy-start.8 = (f32[2048]{0:T(1024)S(1)}, f32[2048]{0:T(1024)}, u32[]{:S(2)}) copy-start(f32[2048]{0:T(1024)} %param.20) | copy-start | bytes 24580
  75.1 83.0 %all-gather.2.cloned.1.call-start = ((), (), s32[]{:S(2)}) async-start(), calls=%async_computation.5 | async-start | bytes 2949120 | tf_op jit(solution)/shard_map/all_gather | solution.py:110
  135.8 79.2 %reduce-scatter.7.cloned.1.call-start = ((), (), s32[]{:S(2)}) async-start(), calls=%async_computation.6 | async-start | bytes 2949120
  167.1 4.7 %copy-start.3 = (bf16[576,2048]{1,0:T(8,128)(2,1)S(1)}, bf16[576,2048]{1,0:T(8,128)(2,1)}, u32[]{:S(2)}) copy-start(bf16[576,2048]{1,0:T(8,128)(2,1)} %reshape.106) | copy-start | bytes 7077892
  167.1 4.8 %copy-start.14 = (bf16[1,2048,768]{2,1,0:T(8,128)(2,1)S(1)}, bf16[1,2048,768]{2,1,0:T(8,128)(2,1)}, u32[]{:S(2)}) copy-start(bf16[1,2048,768]{2,1,0:T(8,128)(2,1)} %param.24) | copy-start | bytes 9437188
  182.0 40.8 %copy-start.13 = (f32[48,2]{0,1:T(2,128)S(1)}, f32[48,2]{0,1:T(2,128)}, u32[]{:S(2)}) copy-start(f32[48,2]{0,1:T(2,128)} %param.22) | copy-start | bytes 1156
  217.3 25.7 %all-to-all-start.1 = ((bf16[8,18,2048]{2,1,0:T(8,128)(2,1)}), bf16[8,18,2048]{2,1,0:T(8,128)(2,1)}, u32[]{:S(2)}, u32[]{:S(2)}) async-start(bf16[8,18,2048]{2,1,0:T(8,128)(2,1)} %copy.63), calls=%async_computation.2 | async-start | bytes 1572864 | tf_op jit(solution)/shard_map/all_to_all | solution.py:126
  245.1 6.7 %copy-start.5 = (bf16[48,2048]{1,0:T(8,128)(2,1)S(1)}, bf16[48,2048]{1,0:T(8,128)(2,1)}, u32[]{:S(2)}) copy-start(bf16[48,2048]{1,0:T(8,128)(2,1)} %reduce-scatter.5.cloned.1.call-done) | copy-start | bytes 589828
Sparse Core Ops, SparseCore 0:
  75.2 24.1 reduce-scatter.4
  135.9 22.1 all-gather.1
  182.1 32.8 reduce-scatter.6
where the time goes:
time: 260 us; the launch traced here: 259 us
  waiting for transfers between devices  97.9 us (38%)
  blocking collectives  61.5 us (24%)
  local copies, waits for them, and re-layouts  51.7 us (20%)
  matrix products  22.6 us (9%)
  between operations  13.5 us (5%)
  other arithmetic  6.16 us (2%)
  starting transfers between devices  5.82 us (2%)
    all_gather x1, blocking collectives, local(): near = lax.all_gather(own_half, 'sp', axis=0, tiled=True)  36 us
    unnamed x4, waiting for transfers between devices  33 us
    all_to_all x1, blocking collectives, local(): lax.all_to_all(outgoing, 'sp', split_axis=0, concat_axis=0, tiled=True)  25.5 us
    reduce_scatter x1, waiting for transfers between devices, local(): lax.psum_scatter(jnp.dot(head_out, w_out, preferred_element_type=jnp.floa...  23.4 us
    all_gather x1, waiting for transfers between devices, local(): lax.all_gather(lax.all_to_all(outgoing, 'sp', split_axis=0, concat_axis=0...  22 us
    all_to_all x1, waiting for transfers between devices, local(): lax.all_to_all(served, 'sp', split_axis=0, concat_axis=0, tiled=True)  19.4 us
    unnamed x47, local copies, waits for them, and re-layouts  8.96 us
    all_to_all x1, starting transfers between devices, local(): lax.all_to_all(served, 'sp', split_axis=0, concat_axis=0, tiled=True)  5.52 us
  transfers between devices with their start and end apart: 5, of which 4 were waited for; matrix products, arithmetic and copies ran while one was open for 3% of the time, Pallas kernels for 0%

commit v1 on v0

--- a/solution.py
+++ b/solution.py
@@ -7,6 +7,22 @@
 KV_HEADS = 2
 EPS = 1e-06
 LOWEST = -1e30
+
+
+def bind_copies(v0, along_axis):
+    world_n = jax.lax.axis_size(along_axis)
+    spare = sorted(((s, (s + 1) % world_n) for s in range(world_n)))
+    met_up = v0
+    ledger = [met_up]
+    tick = 1
+    while tick < world_n:
+        met_up = jax.lax.ppermute(met_up, axis_name=along_axis, perm=spare)
+        ledger.insert(0, met_up)
+        tick += 1
+    val = jnp.concatenate(ledger, 0)
+    all_rows = jax.lax.axis_index(along_axis) + 1
+    built = jnp.roll(val, all_rows * v0.shape[0], 0)
+    return built
 
 
 def swapped(value, axis, apart):
@@ -72,7 +88,7 @@
     part_rows = joined.shape[0] // 2
     side = lax.axis_index("tp") % 2
     own_half = lax.dynamic_slice_in_dim(joined, side * part_rows, part_rows, 0)
-    near = lax.all_gather(own_half, "sp", axis=0, tiled=True)
+    near = bind_copies(own_half, "sp")
     far = swapped(near, "tp", 0)
     high, total, acc = attend(attend(start_state, near, q_heads), far, q_heads)
     mixed = (

time: 260 us -> 284 us (1.092)
  waiting for transfers between devices: 97.9 us -> 144 us
  blocking collectives: 61.5 us -> 25.5 us
  local copies, waits for them, and re-layouts: 51.7 us -> 62.3 us
  starting transfers between devices: 5.82 us -> 8.85 us
    ppermute x0 -> x7, waiting for transfers between devices: none -> 50 us  [bind_copies(): met_up = jax.lax.ppermute(met_up, axis_name=along_axis, perm=spare)]
    all_gather x1 -> x0, blocking collectives: 36 us -> none  [local(): near = lax.all_gather(own_half, 'sp', axis=0, tiled=True)]
    unnamed x47 -> x82, local copies, waits for them, and re-layouts: 8.96 us -> 19 us
    reduce_scatter x1, waiting for transfers between devices: 23.4 us -> 20 us  [local(): lax.psum_scatter(jnp.dot(head_out, w_out, preferred_element_type=jnp.floa...]
    ppermute x0 -> x7, starting transfers between devices: none -> 3.06 us  [bind_copies(): met_up = jax.lax.ppermute(met_up, axis_name=along_axis, perm=spare)]
  transfers between devices with their start and end apart: 5 -> 12, of which waited for: 4 -> 11; matrix products, arithmetic and copies ran while one was open for 3% -> 3% of each run, Pallas kernels for 0% -> 0%
where the time goes in v1:
time: 284 us; the launch traced here: 283 us
  waiting for transfers between devices  144 us (51%)
  local copies, waits for them, and re-layouts  62.3 us (22%)
  blocking collectives  25.5 us (9%)
  matrix products  21.7 us (8%)
  between operations  13.6 us (5%)
  starting transfers between devices  8.85 us (3%)
  other arithmetic  6.16 us (2%)
    ppermute x7, waiting for transfers between devices, bind_copies(): met_up = jax.lax.ppermute(met_up, axis_name=along_axis, perm=spare)  50 us
    unnamed x4, waiting for transfers between devices  33 us
    all_to_all x1, blocking collectives, local(): lax.all_to_all(outgoing, 'sp', split_axis=0, concat_axis=0, tiled=True)  25.5 us
    all_gather x1, waiting for transfers between devices, local(): lax.all_gather(lax.all_to_all(outgoing, 'sp', split_axis=0, concat_axis=0...  22 us
    reduce_scatter x1, waiting for transfers between devices, local(): lax.psum_scatter(jnp.dot(head_out, w_out, preferred_element_type=jnp.floa...  20 us
    all_to_all x1, waiting for transfers between devices, local(): lax.all_to_all(served, 'sp', split_axis=0, concat_axis=0, tiled=True)  19.5 us
    unnamed x82, local copies, waits for them, and re-layouts  19 us
  transfers between devices with their start and end apart: 12, of which 11 were waited for; matrix products, arithmetic and copies ran while one was open for 3% of the time, Pallas kernels for 0%

profile of v1, /device:TPU:0, one launch (start us, length us, event | category | flops | bytes accessed | tf_op | source)
XLA Modules:
  0.0 282.6 jit_solution(382190563640161616)
XLA Ops:
  6.5 1.1 constant_dynamic-slice_fusion.2
  7.7 3.0 %collective-permute-start = (bf16[96,512]{1,0:T(8,128)(2,1)S(1)}, bf16[96,512]{1,0:T(8,128)(2,1)S(1)}, u32[]{:S(2)}, u32[]{:S(2)}) collective-permute-start(bf16[96,512]{1,0:T(8,128)(2,1)S(1)} %fusion.36), channel_id=1, source_target_pairs={{0,4},{4,8},{8,12},{12,16},{16,20},{20,24},{24,28},{28,0},{1,5},{5... | collective-permute-start | bytes 294920 | tf_op jit(solution)/shard_map/ppermute | solution.py:19
  10.7 5.8 %collective-permute-done = bf16[96,512]{1,0:T(8,128)(2,1)S(1)} collective-permute-done((bf16[96,512]{1,0:T(8,128)(2,1)S(1)}, bf16[96,512]{1,0:T(8,128)(2,1)S(1)}, u32[]{:S(2)}, u32[]{:S(2)}) %collective-permute-start) | collective-permute-done | bytes 98336 | tf_op jit(solution)/shard_map/ppermute | solution.py:19
  16.6 7.3 %collective-permute-done.1 = bf16[96,512]{1,0:T(8,128)(2,1)S(1)} collective-permute-done((bf16[96,512]{1,0:T(8,128)(2,1)S(1)}, bf16[96,512]{1,0:T(8,128)(2,1)S(1)}, u32[]{:S(2)}, u32[]{:S(2)}) %collective-permute-start.1) | collective-permute-done | bytes 98336 | tf_op jit(solution)/shard_map/ppermute | solution.py:19
  24.5 7.3 %collective-permute-done.2 = bf16[96,512]{1,0:T(8,128)(2,1)S(1)} collective-permute-done((bf16[96,512]{1,0:T(8,128)(2,1)S(1)}, bf16[96,512]{1,0:T(8,128)(2,1)S(1)}, u32[]{:S(2)}, u32[]{:S(2)}) %collective-permute-start.2) | collective-permute-done | bytes 98336 | tf_op jit(solution)/shard_map/ppermute | solution.py:19
  32.5 7.3 %collective-permute-done.3 = bf16[96,512]{1,0:T(8,128)(2,1)S(1)} collective-permute-done((bf16[96,512]{1,0:T(8,128)(2,1)S(1)}, bf16[96,512]{1,0:T(8,128)(2,1)S(1)}, u32[]{:S(2)}, u32[]{:S(2)}) %collective-permute-start.3) | collective-permute-done | bytes 98336 | tf_op jit(solution)/shard_map/ppermute | solution.py:19
  40.4 7.3 %collective-permute-done.4 = bf16[96,512]{1,0:T(8,128)(2,1)S(1)} collective-permute-done((bf16[96,512]{1,0:T(8,128)(2,1)S(1)}, bf16[96,512]{1,0:T(8,128)(2,1)S(1)}, u32[]{:S(2)}, u32[]{:S(2)}) %collective-permute-start.4) | collective-permute-done | bytes 98336 | tf_op jit(solution)/shard_map/ppermute | solution.py:19
  48.4 8.3 %collective-permute-done.5 = bf16[96,512]{1,0:T(8,128)(2,1)} collective-permute-done((bf16[96,512]{1,0:T(8,128)(2,1)S(1)}, bf16[96,512]{1,0:T(8,128)(2,1)}, u32[]{:S(2)}, u32[]{:S(2)}) %collective-permute-start.5) | collective-permute-done | bytes 98336 | tf_op jit(solution)/shard_map/ppermute | solution.py:19
  56.7 1.0 reshape.102
  57.7 6.6 %collective-permute-done.6 = bf16[96,512]{1,0:T(8,128)(2,1)} collective-permute-done((bf16[96,512]{1,0:T(8,128)(2,1)}, bf16[96,512]{1,0:T(8,128)(2,1)}, u32[]{:S(2)}, u32[]{:S(2)}) %collective-permute-start.6) | collective-permute-done | bytes 98336 | tf_op jit(solution)/shard_map/ppermute | solution.py:19
  64.3 0.9 constant_dynamic-update-slice_fusion.15
  65.2 0.9 constant_dynamic-update-slice_fusion.14
  66.1 0.9 constant_dynamic-update-slice_fusion.13
  67.0 0.9 constant_dynamic-update-slice_fusion.12
  67.9 0.9 constant_dynamic-update-slice_fusion.11
  68.8 0.9 constant_dynamic-update-slice_fusion.10
  69.8 0.9 constant_dynamic-update-slice_fusion.7
  70.7 0.9 constant_dynamic-update-slice_fusion.6
  71.7 1.3 constant_dynamic-slice_fusion.1
  73.6 0.8 constant_dynamic-slice_fusion
  74.5 1.9 copy.43
  76.4 2.9 %bitcast_reduce_fusion.1 = (f32[192,2,2]{0,1,2:T(2,128)S(1)}, f32[2,768,192,2]{1,2,3,0:T(8,128)}) fusion(bf16[768,2,128,1]{0,2,3,1:T(8,128)(2,1)} %bitcast.120, bf16[192,2,2,128]{3,2,1,0:T(2,128)(2,1)S(1)} %reshape.102), kind=kOutput, calls=%fused_computation.16 | convolution fusion | flops 152173824 | bytes 2952192 | tf_op jit(solution)/shard_map/qhmd,kmd->qhmk/dot_general | solution.py:44
  79.3 1.8 slice.34
  81.1 1.9 reshape.103
  82.9 1.6 bitcast_reduce_fusion
  85.2 1.0 copy-done.1
  86.9 1.6 fusion.18
  88.5 1.5 convolution_add_fusion
  90.0 0.9 copy-done.2
  90.9 0.8 slice_bitcast_fusion.2
  91.8 0.8 copy.77
  92.5 1.4 fusion.28
  93.9 0.8 copy.78
  94.7 1.3 copy.53
  96.0 0.8 copy.80
  97.1 0.8 copy.83
  98.4 1.3 div.58.clone
  100.2 1.5 convolution_convert_fusion
  102.7 20.0 %reduce-scatter.5.cloned.1.call-done = bf16[48,2048]{1,0:T(8,128)(2,1)} async-done(((bf16[192,2048]{1,0:T(8,128)(2,1)}), bf16[48,2048]{1,0:T(8,128)(2,1)}) %reduce-scatter.5.cloned.1.call-update) | async-done | bytes 196624 | tf_op jit(solution)/shard_map/reduce_scatter | solution.py:101
  122.7 1.1 multiply_reduce_fusion
  123.8 1.0 multiply_convert_fusion.1
  124.9 1.0 broadcast_in_dim.11
  125.9 1.9 reshape.121
  127.7 2.5 scatter_custom_fusion
  130.3 2.1 reshape.105
  132.4 25.5 %all_to_all.10 = bf16[8,18,2048]{2,1,0:T(8,128)(2,1)S(1)} all-to-all(bf16[8,18,2048]{2,1,0:T(8,128)(2,1)} %reshape.105), channel_id=1, replica_groups=mesh['sp'=8,'tp'=4] {'sp'}, dimensions={0} | all-to-all | bytes 1179648 | tf_op jit(solution)/shard_map/all_to_all | solution.py:127
  157.9 1.1 copy.60
  159.3 22.0 %all-gather.2.cloned.1.call-done = bf16[32,18,2048]{2,0,1:T(8,128)(2,1)} async-done(((bf16[8,18,2048]{2,0,1:T(8,128)(2,1)}), bf16[32,18,2048]{2,0,1:T(8,128)(2,1)}) %all-gather.2.cloned.1.call-update) | async-done | bytes 2359312 | tf_op jit(solution)/shard_map/all_gather | solution.py:126
  181.3 4.7 %copy.61 = bf16[32,18,2048]{2,1,0:T(8,128)(2,1)} copy(bf16[32,18,2048]{2,0,1:T(8,128)(2,1)} %all-gather.2.cloned.1.call-done) | data formatting | bytes 4718592 | tf_op jit(solution)/shard_map/all_gather | solution.py:126
  186.0 4.3 %reshape.106 = bf16[576,2048]{1,0:T(8,128)(2,1)} reshape(bf16[32,18,2048]{2,1,0:T(8,128)(2,1)} %copy.61) | data formatting | bytes 4718592 | tf_op jit(solution)/shard_map/reshape | solution.py:132
  190.3 4.7 %fusion.4 = f32[576,768]{1,0:T(8,128)S(1)} fusion(bf16[576,2048]{1,0:T(8,128)(2,1)} %reshape.106, bf16[1,2048,768]{2,1,0:T(8,128)(2,1)} %param.23), kind=kOutput, calls=%fused_computation.6 | convolution fusion | flops 1811939328 | bytes 7274496 | tf_op jit(solution)/shard_map/dot_general | solution.py:133
  195.1 3.0 %multiply_convert_fusion = bf16[576,768]{1,0:T(8,128)(2,1)} fusion(f32[576,768]{1,0:T(8,128)S(1)} %fusion.4, bf16[576,2048]{1,0:T(8,128)(2,1)S(1)} %copy-done.3, bf16[1,2048,768]{2,1,0:T(8,128)(2,1)S(1)} %copy-done.24), kind=kOutput, calls=%fused_computation.21 | convolution fusion | flops 1814593536 | bytes 8159232 | tf_op jit(solution)/shard_map/dot_general | solution.py:134
  198.2 2.3 dot_general.36
  200.4 3.3 %fusion.9 = bf16[18,4,8,2048]{3,2,1,0:T(8,128)(2,1)S(1)} fusion(bf16[1,768,2048]{2,1,0:T(8,128)(2,1)S(1)} %copy-done, bf16[32,18,768]{2,1,0:T(8,128)(2,1)} %dot_general.36), kind=kOutput, calls=%fused_computation.9 | convolution fusion | flops 1813118976 | bytes 6389760 | tf_op jit(solution)/shard_map/dot_general | solution.py:136
  203.7 1.6 copy.79
  205.3 33.0 %reduce-scatter.7.cloned.1.call-done = bf16[8,36864]{1,0:T(8,128)(2,1)} async-done(((bf16[32,36864]{1,0:T(8,128)(2,1)}), bf16[8,36864]{1,0:T(8,128)(2,1)}) %reduce-scatter.7.cloned.1.call-update) | async-done | bytes 589840
  238.3 2.3 copy.63
  240.6 5.5 %all-to-all-start.1 = ((bf16[8,18,2048]{2,1,0:T(8,128)(2,1)}), bf16[8,18,2048]{2,1,0:T(8,128)(2,1)}, u32[]{:S(2)}, u32[]{:S(2)}) async-start(bf16[8,18,2048]{2,1,0:T(8,128)(2,1)} %copy.63), calls=%async_computation.2 | async-start | bytes 1572864 | tf_op jit(solution)/shard_map/all_to_all | solution.py:142
  246.9 19.5 %all-to-all-done.1 = bf16[8,18,2048]{2,1,0:T(8,128)(2,1)} async-done(((bf16[8,18,2048]{2,1,0:T(8,128)(2,1)}), bf16[8,18,2048]{2,1,0:T(8,128)(2,1)}, u32[]{:S(2)}, u32[]{:S(2)}) %all-to-all-start.1) | async-done | bytes 589856 | tf_op jit(solution)/shard_map/all_to_all | solution.py:142
  266.3 2.2 reshape.107
  268.5 3.1 %gather_fusion = bf16[96,2048]{1,0:T(8,128)(2,1)} fusion(bf16[144,2048]{1,0:T(8,128)(2,1)} %reshape.107, s32[1024]{0:T(1024)S(1)} %pad_clamp_fusion), kind=kCustom, calls=%fused_computation | custom fusion | bytes 786816 | tf_op jit(solution)/shard_map/gather | solution.py:145
  271.6 2.0 reshape.108
  273.6 1.5 fusion.42
  275.2 0.8 fusion.24
  (104 shorter events, 7.8 us)
Async XLA Ops:
  6.5 193.9 %copy-start = (bf16[1,768,2048]{2,1,0:T(8,128)(2,1)S(1)}, bf16[1,768,2048]{2,1,0:T(8,128)(2,1)}, u32[]{:S(2)}) copy-start(bf16[1,768,2048]{2,1,0:T(8,128)(2,1)} %param.25) | copy-start | bytes 9437188
  6.5 116.2 %reduce-scatter.5.cloned.1.call-start = ((), (), s32[]{:S(2)}) async-start(), calls=%async_computation.4 | async-start | bytes 983040 | tf_op jit(solution)/shard_map/reduce_scatter | solution.py:101
  7.7 8.9 %collective-permute-start = (bf16[96,512]{1,0:T(8,128)(2,1)S(1)}, bf16[96,512]{1,0:T(8,128)(2,1)S(1)}, u32[]{:S(2)}, u32[]{:S(2)}) collective-permute-start(bf16[96,512]{1,0:T(8,128)(2,1)S(1)} %fusion.36), channel_id=1, source_target_pairs={{0,4},{4,8},{8,12},{12,16},{16,20},{20,24},{24,28},{28,0},{1,5},{5... | collective-permute-start | bytes 294920 | tf_op jit(solution)/shard_map/ppermute | solution.py:19
  16.6 7.3 %collective-permute-start.1 = (bf16[96,512]{1,0:T(8,128)(2,1)S(1)}, bf16[96,512]{1,0:T(8,128)(2,1)S(1)}, u32[]{:S(2)}, u32[]{:S(2)}) collective-permute-start(bf16[96,512]{1,0:T(8,128)(2,1)S(1)} %collective-permute-done), channel_id=1, source_target_pairs={{0,4},{4,8},{8,12},{12,16},{16,20},{20,24},{24,28},{28,0},{1,5},{5... | collective-permute-start | bytes 294920 | tf_op jit(solution)/shard_map/ppermute | solution.py:19
  23.9 0.6 copy-start.9
  24.5 7.3 %collective-permute-start.2 = (bf16[96,512]{1,0:T(8,128)(2,1)S(1)}, bf16[96,512]{1,0:T(8,128)(2,1)S(1)}, u32[]{:S(2)}, u32[]{:S(2)}) collective-permute-start(bf16[96,512]{1,0:T(8,128)(2,1)S(1)} %collective-permute-done.1), channel_id=1, source_target_pairs={{0,4},{4,8},{8,12},{12,16},{16,20},{20,24},{24,28},{28,0},{1,5},{5... | collective-permute-start | bytes 294920 | tf_op jit(solution)/shard_map/ppermute | solution.py:19
  31.8 0.6 copy-start.11
  32.5 7.3 %collective-permute-start.3 = (bf16[96,512]{1,0:T(8,128)(2,1)S(1)}, bf16[96,512]{1,0:T(8,128)(2,1)S(1)}, u32[]{:S(2)}, u32[]{:S(2)}) collective-permute-start(bf16[96,512]{1,0:T(8,128)(2,1)S(1)} %collective-permute-done.2), channel_id=1, source_target_pairs={{0,4},{4,8},{8,12},{12,16},{16,20},{20,24},{24,28},{28,0},{1,5},{5... | collective-permute-start | bytes 294920 | tf_op jit(solution)/shard_map/ppermute | solution.py:19
  39.8 0.6 copy-start.13
  40.4 7.3 %collective-permute-start.4 = (bf16[96,512]{1,0:T(8,128)(2,1)S(1)}, bf16[96,512]{1,0:T(8,128)(2,1)S(1)}, u32[]{:S(2)}, u32[]{:S(2)}) collective-permute-start(bf16[96,512]{1,0:T(8,128)(2,1)S(1)} %collective-permute-done.3), channel_id=1, source_target_pairs={{0,4},{4,8},{8,12},{12,16},{16,20},{20,24},{24,28},{28,0},{1,5},{5... | collective-permute-start | bytes 294920 | tf_op jit(solution)/shard_map/ppermute | solution.py:19
  47.7 0.6 copy-start.15
  48.4 8.3 %collective-permute-start.5 = (bf16[96,512]{1,0:T(8,128)(2,1)S(1)}, bf16[96,512]{1,0:T(8,128)(2,1)}, u32[]{:S(2)}, u32[]{:S(2)}) collective-permute-start(bf16[96,512]{1,0:T(8,128)(2,1)S(1)} %collective-permute-done.4), channel_id=1, source_target_pairs={{0,4},{4,8},{8,12},{12,16},{16,20},{20,24},{24,28},{28,0},{1,5},{5... | collective-permute-start | bytes 294920 | tf_op jit(solution)/shard_map/ppermute | solution.py:19
  56.7 7.6 %collective-permute-start.6 = (bf16[96,512]{1,0:T(8,128)(2,1)}, bf16[96,512]{1,0:T(8,128)(2,1)}, u32[]{:S(2)}, u32[]{:S(2)}) collective-permute-start(bf16[96,512]{1,0:T(8,128)(2,1)} %collective-permute-done.5), channel_id=1, source_target_pairs={{0,4},{4,8},{8,12},{12,16},{16,20},{20,24},{24,28},{28,0},{1,5},{5... | collective-permute-start | bytes 294920 | tf_op jit(solution)/shard_map/ppermute | solution.py:19
  57.7 13.9 %copy-start.16 = (bf16[96,512]{1,0:T(8,128)(2,1)S(1)}, bf16[96,512]{1,0:T(8,128)(2,1)}, u32[]{:S(2)}) copy-start(bf16[96,512]{1,0:T(8,128)(2,1)} %copy-done.15) | copy-start | bytes 294916
  57.7 13.9 %copy-start.14 = (bf16[96,512]{1,0:T(8,128)(2,1)S(1)}, bf16[96,512]{1,0:T(8,128)(2,1)}, u32[]{:S(2)}) copy-start(bf16[96,512]{1,0:T(8,128)(2,1)} %copy-done.13) | copy-start | bytes 294916
  57.7 13.9 %copy-start.12 = (bf16[96,512]{1,0:T(8,128)(2,1)S(1)}, bf16[96,512]{1,0:T(8,128)(2,1)}, u32[]{:S(2)}) copy-start(bf16[96,512]{1,0:T(8,128)(2,1)} %copy-done.11) | copy-start | bytes 294916
  57.7 13.9 %copy-start.10 = (bf16[96,512]{1,0:T(8,128)(2,1)S(1)}, bf16[96,512]{1,0:T(8,128)(2,1)}, u32[]{:S(2)}) copy-start(bf16[96,512]{1,0:T(8,128)(2,1)} %copy-done.9) | copy-start | bytes 294916
  69.7 3.3 %copy-start.21 = (f32[2]{0:T(128)S(1)}, f32[2]{0:T(128)}, u32[]{:S(2)}) copy-start(f32[2]{0:T(128)} %param.16) | copy-start | bytes 28
  69.7 3.3 %copy-start.22 = (f32[256]{0:T(256)S(1)}, f32[256]{0:T(256)}, u32[]{:S(2)}) copy-start(f32[256]{0:T(256)} %param.17) | copy-start | bytes 3076
  71.7 1.9 copy-start.6
  73.0 6.3 %collective-permute-start.7 = (bf16[768,512]{1,0:T(8,128)(2,1)}, bf16[768,512]{1,0:T(8,128)(2,1)}, u32[]{:S(2)}, u32[]{:S(2)}) collective-permute-start(bf16[768,512]{1,0:T(8,128)(2,1)} %constant_dynamic-slice_fusion.1), channel_id=1, source_target_pairs={{0,1},{1,0},{2,3},{3,2},{4,5},{5,4},{6,7},{7,6},{8,9},{9,8},{10,11... | collective-permute-start | bytes 2359304 | tf_op jit(solution)/shard_map/ppermute | solution.py:31
  84.5 1.7 copy-start.1
  90.0 0.9 copy-start.2
  97.1 2.6 copy-start.17
  98.3 1.7 copy-start.7
  98.3 1.7 copy-start.8
  98.3 1.7 copy-start.20
  98.3 1.9 copy-start.25
  100.2 1.6 copy-start.19
  100.2 22.5 %copy-start.4 = (bf16[48,2048]{1,0:T(8,128)(2,1)S(1)}, bf16[48,2048]{1,0:T(8,128)(2,1)}, u32[]{:S(2)}) copy-start(bf16[48,2048]{1,0:T(8,128)(2,1)} %param.19) | copy-start | bytes 589828
  100.2 23.6 %copy-start.18 = (f32[2048]{0:T(1024)S(1)}, f32[2048]{0:T(1024)}, u32[]{:S(2)}) copy-start(f32[2048]{0:T(1024)} %param.20) | copy-start | bytes 24580
  101.8 79.5 %all-gather.2.cloned.1.call-start = ((), (), s32[]{:S(2)}) async-start(), calls=%async_computation.5 | async-start | bytes 2949120 | tf_op jit(solution)/shard_map/all_gather | solution.py:126
  159.0 79.2 %reduce-scatter.7.cloned.1.call-start = ((), (), s32[]{:S(2)}) async-start(), calls=%async_computation.6 | async-start | bytes 2949120
  190.3 4.7 %copy-start.3 = (bf16[576,2048]{1,0:T(8,128)(2,1)S(1)}, bf16[576,2048]{1,0:T(8,128)(2,1)}, u32[]{:S(2)}) copy-start(bf16[576,2048]{1,0:T(8,128)(2,1)} %reshape.106) | copy-start | bytes 7077892
  190.3 4.8 %copy-start.24 = (bf16[1,2048,768]{2,1,0:T(8,128)(2,1)S(1)}, bf16[1,2048,768]{2,1,0:T(8,128)(2,1)}, u32[]{:S(2)}) copy-start(bf16[1,2048,768]{2,1,0:T(8,128)(2,1)} %param.24) | copy-start | bytes 9437188
  205.3 40.8 %copy-start.23 = (f32[48,2]{0,1:T(2,128)S(1)}, f32[48,2]{0,1:T(2,128)}, u32[]{:S(2)}) copy-start(f32[48,2]{0,1:T(2,128)} %param.22) | copy-start | bytes 1156
  240.6 25.7 %all-to-all-start.1 = ((bf16[8,18,2048]{2,1,0:T(8,128)(2,1)}), bf16[8,18,2048]{2,1,0:T(8,128)(2,1)}, u32[]{:S(2)}, u32[]{:S(2)}) async-start(bf16[8,18,2048]{2,1,0:T(8,128)(2,1)} %copy.63), calls=%async_computation.2 | async-start | bytes 1572864 | tf_op jit(solution)/shard_map/all_to_all | solution.py:142
  271.6 3.6 %copy-start.5 = (bf16[48,2048]{1,0:T(8,128)(2,1)S(1)}, bf16[48,2048]{1,0:T(8,128)(2,1)}, u32[]{:S(2)}) copy-start(bf16[48,2048]{1,0:T(8,128)(2,1)} %reduce-scatter.5.cloned.1.call-done) | copy-start | bytes 589828
Sparse Core Ops, SparseCore 0:
  101.9 20.7 reduce-scatter.4
  159.2 22.1 all-gather.1
  205.4 32.8 reduce-scatter.6
